TPU v7x, 32 devices: a whole 2x2x4 slice. The times are simulated.
32 devices in a mesh: sp: 4 (over z), fs: 4 (over y, x), tp: 2 (over core).
Axes of the slice: x: 2, y: 2, z: 4, core: 2. Of those that a mesh axis runs over, the one named last changes fastest.
Arguments:
- tokens: bfloat16 [16384, 2048], P(('fs', 'sp', 'tp')), parts along dimension 0, may hold values from -6 to 6
- norm_gain: float32 [2048], replicated, may hold values from 0.1 to 1.9
- w_pool: bfloat16 [2048, 1024], P(None, 'tp'), may hold values from -0.125 to 0.125
- w_query: bfloat16 [2048, 1024], P(None, 'tp'), may hold values from -0.125 to 0.125
- w_key: bfloat16 [2048, 1024], P(None, 'tp'), may hold values from -0.125 to 0.125
- w_value: bfloat16 [2048, 1024], P(None, 'tp'), may hold values from -0.125 to 0.125
- w_gate: bfloat16 [2048, 1024], P(None, 'tp'), may hold values from -0.125 to 0.125
- pool_mix: bfloat16 [4, 256, 256], P('tp'), may hold values from -0.375 to 0.375
- pool_bias: float32 [4, 256], P('tp'), may hold values from -3 to 3
- pool_gain: float32 [1024], P('tp'), may hold values from 0.1 to 1.9
- ret_gain: float32 [1024], P('tp'), may hold values from 0.1 to 1.9
- w_out_pool: bfloat16 [1024, 2048], P('tp'), may hold values from -0.125 to 0.125
- w_out_ret: bfloat16 [1024, 2048], P('tp'), may hold values from -0.125 to 0.125
Outputs:
- mixed: bfloat16 [16384, 2048], P(('fs', 'sp', 'tp')), parts along dimension 0
There are 4 independent parts, one for each index of `fs`. A program takes and returns all parts, laid end to end along the dimension named above; an argument that names none is the same for every part. Nothing has to cross between parts.
All inputs are finite; a program needn't handle non-finite values.
Results may differ from a plain program's by a relative error of at most 0.012.
Values may be sent and summed in bfloat16 or wider, within the bound.
A program may use at most 128 MiB of HBM per device.

v0:
```python
import jax
import jax.numpy as jnp
from jax import lax
from jax.sharding import PartitionSpec as P

GROUP_DIM = 256
HEAD_DIM = 128
BLOCK = 128


rim_len = 16


def shifted(array, axis, by):
    length = lax.axis_size(axis)
    pairs = [(i, i + by) for i in range(length) if 0 <= i + by < length]
    return lax.ppermute(array, axis, pairs)


def rotary(values, positions):
    half = values.shape[-1] // 2
    inverse = 10000.0 ** (-jnp.arange(half, dtype=jnp.float32) / half)
    angles = positions[:, None] * inverse[None, :]
    cosine = jnp.cos(angles)[:, None, :]
    sine = jnp.sin(angles)[:, None, :]
    first = values[..., :half]
    second = values[..., half:]
    return jnp.concatenate(
        [first * cosine - second * sine, second * cosine + first * sine], axis=-1
    )


def retain(query, key, value, log_decay):
    length, heads_here = (query.shape[0], query.shape[1])
    blocks = length // BLOCK
    hp = lax.Precision.HIGHEST

    def split(values):
        return values.reshape(blocks, BLOCK, heads_here, HEAD_DIM).transpose(0, 2, 1, 3)

    steps = jnp.arange(BLOCK, dtype=jnp.float32)
    apart = steps[:, None] - steps[None, :]
    inner = jnp.where(
        apart[None] >= 0, jnp.exp(log_decay[:, None, None] * jnp.maximum(apart, 0.0)[None]), 0.0
    )
    query_decay = jnp.exp(log_decay[:, None] * (steps[None, :] + 1.0))
    key_decay = jnp.exp(log_decay[:, None] * (BLOCK - 1.0 - steps[None, :]))
    block_decay = jnp.exp(log_decay * BLOCK)

    def advance(state, pieces):
        qb, kb, vb = pieces
        scores = jnp.einsum("hid,hjd->hij", qb, kb, precision=hp) * inner
        out = jnp.einsum("hij,hje->hie", scores, vb, precision=hp)
        out = out + jnp.einsum("hid,hde->hie", qb, state, precision=hp) * query_decay[:, :, None]
        state = state * block_decay[:, None, None] + jnp.einsum(
            "hjd,hje->hde", kb * key_decay[:, :, None], vb, precision=hp
        )
        return (state, out)

    start = jnp.zeros((heads_here, HEAD_DIM, HEAD_DIM), jnp.float32)
    state, outs = lax.scan(advance, start, (split(query), split(key), split(value)))
    return (outs.transpose(0, 2, 1, 3).reshape(length, heads_here, HEAD_DIM), state)


def per_device(
    tokens,
    norm_gain,
    w_pool,
    w_query,
    w_key,
    w_value,
    w_gate,
    pool_mix,
    pool_bias,
    pool_gain,
    ret_gain,
    w_out_pool,
    w_out_ret,
):
    tp_index = lax.axis_index("tp")
    sp_index = lax.axis_index("sp")
    xf = tokens.astype(jnp.float32)
    normed = (xf * lax.rsqrt(jnp.mean(xf * xf, axis=-1, keepdims=True) + 1e-06) * norm_gain).astype(
        jnp.bfloat16
    )
    weights = (w_pool, w_query, w_key, w_value, w_gate)
    piece = lax.all_gather(normed, "tp", axis=0, tiled=True)
    projected = jnp.concatenate(
        [
            jnp.dot(piece, weight, preferred_element_type=jnp.float32).astype(jnp.bfloat16)
            for weight in weights
        ],
        axis=1,
    )
    width_pool = w_pool.shape[1]
    width_ret = w_query.shape[1]
    pool_in = projected[:, :width_pool]
    query = projected[:, width_pool : width_pool + width_ret]
    key = projected[:, width_pool + width_ret : width_pool + 2 * width_ret]
    value = projected[:, width_pool + 2 * width_ret : width_pool + 3 * width_ret]
    gate = projected[:, width_pool + 3 * width_ret :]
    length = projected.shape[0]
    seq_len = length * lax.axis_size("sp")
    positions = (sp_index * length + jnp.arange(length, dtype=jnp.int32)).astype(jnp.float32)
    heads_here = width_ret // HEAD_DIM
    total_heads = heads_here * lax.axis_size("tp")
    head_ids = (tp_index * heads_here + jnp.arange(heads_here, dtype=jnp.int32)).astype(jnp.float32)
    log_decay = -(2.0 ** (-5)) * (seq_len / 16.0) ** (-2.0 * head_ids / (total_heads - 1))
    qf = rotary(query.astype(jnp.float32).reshape(length, heads_here, HEAD_DIM), positions)
    kf = rotary(
        key.astype(jnp.float32).reshape(length, heads_here, HEAD_DIM), positions
    ) * HEAD_DIM ** (-0.5)
    vf = value.astype(jnp.float32).reshape(length, heads_here, HEAD_DIM)
    local_out, local_state = retain(qf, kf, vf, log_decay)
    device_decay = jnp.exp(log_decay * length)
    empty_state = jnp.zeros_like(local_state)

    def relay(turn, carried):
        incoming, outgoing = carried
        incoming = shifted(outgoing.astype(jnp.bfloat16), "sp", 1).astype(outgoing.dtype)
        return (incoming, local_state + device_decay[:, None, None] * incoming)

    incoming, passed = lax.fori_loop(0, lax.axis_size("sp") - 1, relay, (empty_state, local_state))
    rim = shifted(pool_in[length - rim_len :], "sp", 1)
    padded = jnp.concatenate([rim, pool_in], axis=0).astype(jnp.float32)
    groups_here = width_pool // GROUP_DIM
    group_local = jnp.arange(width_pool, dtype=jnp.int32) // GROUP_DIM
    window = jnp.power(2, 1 + tp_index * groups_here + group_local)
    window_sum = jnp.zeros((length, width_pool), jnp.float32)
    for offset in range(rim_len):
        window_sum = window_sum + jnp.where(
            offset < window[None, :], padded[rim_len - offset : rim_len - offset + length], 0.0
        )
    count = jnp.minimum(positions[:, None] + 1.0, window[None, :].astype(jnp.float32))
    diff = (
        (window_sum / count - padded[rim_len:])
        .astype(jnp.bfloat16)
        .reshape(length, groups_here, GROUP_DIM)
    )
    mixed_groups = (
        jnp.einsum("lgc,gcd->lgd", diff, pool_mix, preferred_element_type=jnp.float32)
        + pool_bias[None]
    )
    pool_out = (mixed_groups.reshape(length, width_pool) * pool_gain[None, :]).astype(jnp.bfloat16)
    local_steps = jnp.arange(length, dtype=jnp.float32)
    carry_decay = jnp.exp(log_decay[None, :] * (local_steps[:, None] + 1.0))
    raw = local_out + jnp.einsum(
        "lhd,hde->lhe", qf * carry_decay[:, :, None], incoming, precision=lax.Precision.HIGHEST
    )
    mean = jnp.mean(raw, axis=-1, keepdims=True)
    var = jnp.mean(jnp.square(raw - mean), axis=-1, keepdims=True)
    normalized = ((raw - mean) * lax.rsqrt(var + 1e-06)).reshape(length, width_ret) * ret_gain[
        None, :
    ]
    ret_out = (jax.nn.silu(gate.astype(jnp.float32)) * normalized).astype(jnp.bfloat16)
    summed = jnp.dot(pool_out, w_out_pool, preferred_element_type=jnp.float32) + jnp.dot(
        ret_out, w_out_ret, preferred_element_type=jnp.float32
    )
    rounded = lax.optimization_barrier(summed.astype(jnp.bfloat16))
    return lax.psum_scatter(
        rounded.astype(jnp.float32).astype(jnp.bfloat16), "tp", scatter_dimension=0, tiled=True
    )


def solution(mesh):
    return jax.shard_map(
        per_device,
        mesh=mesh,
        in_specs=(
            P(("fs", "sp", "tp"), None),
            P(),
            P(None, "tp"),
            P(None, "tp"),
            P(None, "tp"),
            P(None, "tp"),
            P(None, "tp"),
            P("tp", None, None),
            P("tp", None),
            P("tp"),
            P("tp"),
            P("tp", None),
            P("tp", None),
        ),
        out_specs=P(("fs", "sp", "tp"), None),
        check_vma=False,
    )
```

profile of v0, /device:TPU:29, one launch (start us, length us, event | category | flops | bytes accessed | tf_op | source)
XLA Modules:
  0.0 236.2 jit_solution(2249466856135327917)
XLA Ops:
  16.9 3.1 %multiply_cosine_fusion = (f32[1024,64]{1,0:T(8,128)}, f32[1024,64]{1,0:T(8,128)}) fusion(f32[64]{0:T(128)S(1)} %multiply_power_fusion, f32[1024]{0:T(1024)S(1)} %add_convert_fusion.1), kind=kLoop, calls=%fused_computation.109 | loop fusion | flops 65536 | bytes 528640 | tf_op jit(solution)/shard_map/cos | solution.py:24
  20.1 6.9 %all-gather.2.cloned.1.call-done = bf16[1024,2048]{1,0:T(8,128)(2,1)} async-done(((bf16[512,2048]{1,0:T(8,128)(2,1)}), bf16[1024,2048]{1,0:T(8,128)(2,1)}) %all-gather.2.cloned.1.call-update) | async-done | bytes 4194320 | tf_op jit(solution)/shard_map/all_gather | solution.py:87
  27.0 5.3 %convolution_convert_fusion.4 = bf16[1024,512]{1,0:T(8,128)(2,1)S(1)} fusion(bf16[1024,2048]{1,0:T(8,128)(2,1)} %all-gather.2.cloned.1.call-done, bf16[2048,512]{1,0:T(8,128)(2,1)} %param.19), kind=kOutput, calls=%fused_computation.103 | convolution fusion | flops 2148007936 | bytes 7340032 | tf_op jit(solution)/shard_map/dot_general | solution.py:90
  37.5 3.2 %copy.46 = f32[1024,4,64]{2,0,1:T(8,128)} copy(f32[1024,4,64]{0,2,1:T(8,128)} %get-tuple-element.278) | data formatting | bytes 2097152
  40.7 5.2 %convolution_convert_fusion = bf16[1024,512]{0,1:T(8,128)(2,1)S(1)} fusion(bf16[1024,2048]{1,0:T(8,128)(2,1)} %all-gather.2.cloned.1.call-done, bf16[2048,512]{1,0:T(8,128)(2,1)} %param.20), kind=kOutput, calls=%fused_computation.98 | convolution fusion | flops 2148007936 | bytes 7340032 | tf_op jit(solution)/shard_map/dot_general | solution.py:90
  47.5 3.2 %copy.48 = f32[1024,4,64]{2,0,1:T(8,128)} copy(f32[1024,4,64]{0,2,1:T(8,128)} %get-tuple-element.276) | data formatting | bytes 2097152
  50.6 3.2 %copy.47 = f32[1024,4,64]{2,0,1:T(8,128)} copy(f32[1024,4,64]{0,2,1:T(8,128)} %get-tuple-element.277) | data formatting | bytes 2097152
  55.9 7.5 %multiply_subtract_fusion = (f32[1024,4,64]{2,0,1:T(8,128)}, f32[1024,4,64]{2,0,1:T(8,128)}, f32[1024,4,64]{2,0,1:T(8,128)}, f32[1024,4,64]{2,0,1:T(8,128)}) fusion(f32[1024,4,64]{2,0,1:T(8,128)} %copy.48, f32[1024,4,64]{2,0,1:T(8,128)} %copy.47, f32[1024,64]{1,0:T(8,128)} %get-tuple-element.281, f32[1024,64]{1,0:T(8,128)} %get-tuple-element.280, ...), kind=kLoop, calls=%fused_computation.91 | loop fusion | flops 3145728 | bytes 8912896 | tf_op jit(solution)/shard_map/sub | solution.py:29
  65.6 3.1 %copy.40 = f32[8,128,4,64]{1,0,3,2:T(8,128)} copy(f32[8,128,4,64]{3,1,0,2:T(8,128)} %bitcast.89) | data formatting | bytes 2097152 | tf_op jit(solution)/shard_map/concatenate | solution.py:28
  68.8 6.6 %fusion.64 = f32[1024,512]{1,0:T(8,128)} fusion(bf16[1024,2048]{1,0:T(8,128)(2,1)} %all-gather.2.cloned.1.call-done, bf16[2048,512]{1,0:T(8,128)(2,1)} %param.22), kind=kOutput, calls=%fused_computation.100 | convolution fusion | flops 2148532224 | bytes 8388608 | tf_op jit(solution)/shard_map/dot_general | solution.py:90
  75.3 3.0 %reshape.331 = f32[8,128,4,128]{3,2,1,0:T(4,128)} reshape(f32[1024,512]{1,0:T(8,128)} %fusion.64) | data formatting | bytes 4194304 | tf_op jit(solution)/shard_map/transpose | solution.py:39
  78.3 3.4 %copy.55 = f32[8,128,4,128]{3,1,2,0:T(8,128)} copy(f32[8,128,4,128]{3,2,1,0:T(4,128)} %reshape.331) | data formatting | bytes 4194304 | tf_op jit(solution)/shard_map/transpose | solution.py:39
  85.1 64.4 %while.29 = (s32[]{:T(128)}, f32[4,128,128]{2,1,0:T(8,128)S(1)}, f32[8,4,128,128]{3,2,1,0:T(8,128)}, f32[8,4,128,128]{2,0,3,1:T(8,128)}, f32[8,4,128,128]{3,2,1,...) while((s32[]{:T(128)}, f32[4,128,128]{2,1,0:T(8,128)S(1)}, ...), condition=%wide.region_2.3_spmd.clone.clone.clone, body=%wide.region_1.2_spmd.clone.clone.clone.sunk | while | flops 403309568 | bytes 4287211 | solution.py:61
  149.6 2.9 %copy.35 = f32[8,128,4,128]{1,0,3,2:T(8,128)} copy(f32[8,128,4,128]{3,1,2,0:T(8,128)} %bitcast.95) | data formatting | bytes 4194304 | tf_op jit(solution)/shard_map/transpose | solution.py:62
  155.2 21.0 %while.28 = (s32[]{:T(128)}, f32[4,128,128]{2,1,0:T(8,128)}, bf16[4,128,128]{2,1,0:T(8,128)(2,1)S(1)}, f32[4,128,128]{2,1,0:T(8,128)S(1)}, s32[]{:T(128)}, /*index=5*/s32[]{:T(128)}) while((s32[]{:T(128)}, f32[4,128,128]{2,1,0:T(8,128)}, bf16[4,128,128]{2,1,0:T(8,128)(2,1)S(1)}, f32[4,128,128]{2,1,0:T(8,128)S(1)}, s32[]{:T(128)}, ...), condition=%wide.region_4.5_spmd.clone, body=%wide.region_3.4_spmd.clone.sunk | while | flops 262162 | bytes 1310865 | solution.py:123
  156.5 6.0 %collective-permute-done = bf16[4,128,128]{2,1,0:T(8,128)(2,1)S(1)} collective-permute-done((bf16[4,128,128]{2,1,0:T(8,128)(2,1)S(1)}, bf16[4,128,128]{2,1,0:T(8,128)(2,1)S(1)}, u32[]{:S(2)}, u32[]{:S(2)}) %collective-permute-start) | collective-permute-done | bytes 131104 | tf_op jit(solution)/shard_map/while/body/eval_jaxpr/ppermute | solution.py:17
  164.6 4.4 %collective-permute-done = bf16[4,128,128]{2,1,0:T(8,128)(2,1)S(1)} collective-permute-done((bf16[4,128,128]{2,1,0:T(8,128)(2,1)S(1)}, bf16[4,128,128]{2,1,0:T(8,128)(2,1)S(1)}, u32[]{:S(2)}, u32[]{:S(2)}) %collective-permute-start) | collective-permute-done | bytes 131104 | tf_op jit(solution)/shard_map/while/body/eval_jaxpr/ppermute | solution.py:17
  171.1 4.4 %collective-permute-done = bf16[4,128,128]{2,1,0:T(8,128)(2,1)S(1)} collective-permute-done((bf16[4,128,128]{2,1,0:T(8,128)(2,1)S(1)}, bf16[4,128,128]{2,1,0:T(8,128)(2,1)S(1)}, u32[]{:S(2)}, u32[]{:S(2)}) %collective-permute-start) | collective-permute-done | bytes 131104 | tf_op jit(solution)/shard_map/while/body/eval_jaxpr/ppermute | solution.py:17
  176.2 4.9 %fusion.79 = (f32[1024,4]{0,1:T(4,128)S(1)}, f32[1024,4,128]{0,2,1:T(8,128)S(1)}) fusion(f32[1024,4,128]{0,2,1:T(8,128)} %reshape.325, f32[4,128,128]{2,1,0:T(8,128)} %get-tuple-element.86, f32[1024,4,128]{2,0,1:T(8,128)} %bitcast.87, f32[1024,4]{0,1:T(4,128)S(1)} %multiply_exponential_fusion.4), kind=kOutput, calls=%fused_computation.163 | convolution fusion | flops 806875136 | bytes 6586368 | tf_op jit(solution)/shard_map/lhd,hde->lhe/dot_general | solution.py:147
  183.0 3.0 %copy.42 = f32[1024,512]{1,0:T(8,128)} copy(f32[1024,512]{0,1:T(8,128)} %bitcast.91) | data formatting | bytes 4194304 | tf_op jit(solution)/shard_map/reshape | solution.py:152
  186.8 6.1 %fusion.61 = bf16[1024,512]{1,0:T(8,128)(2,1)S(1)} fusion(f32[1040,512]{1,0:T(8,128)S(1)} %maximum_convert_fusion, f32[512]{0:T(512)S(1)} %copy-done.8, f32[1024]{0:T(1024)S(1)} %broadcast_add_fusion, pred[512]{0:T(512)(128)(4,1)S(1)} %copy-done.23, pred[512]{0:T(512)(128)(4,1)S(1)} %copy-done.24, pred[512]{0:T(512)(128)(4,1)S(1)} %copy-done.19, ...), kind=kLoop, calls=%fused_computation.95 | loop fusion | flops 18350080 | bytes 34617344 | tf_op jit(solution)/shard_map/convert_element_type | solution.py:137
  193.8 5.7 %fusion.80 = f32[1024,2048]{1,0:T(8,128)} fusion(bf16[1024,512]{0,1:T(8,128)(2,1)S(1)} %fusion.57, bf16[512,2048]{1,0:T(8,128)(2,1)S(1)} %copy-done), kind=kOutput, calls=%fused_computation.164 | convolution fusion | flops 2147483648 | bytes 11534336 | tf_op jit(solution)/shard_map/dot_general | solution.py:156
  199.5 13.1 %add_convert_fusion = bf16[1024,2048]{1,0:T(8,128)(2,1)} fusion(f32[1024,2048]{1,0:T(8,128)} %fusion.80, bf16[512,2048]{1,0:T(8,128)(2,1)} %param.29, f32[1024,512]{1,0:T(8,128)} %copy.42, bf16[1024,2048]{1,0:T(8,128)(2,1)} %all-gather.2.cloned.1.call-done, bf16[2048,512]{1,0:T(8,128)(2,1)} %param.23, f32[512]{0:T(512)S(1)} %copy-done.29), kind=kOutput, calls=%fused_computation.36 | convolution fusion | flops 4303880192 | bytes 23070720 | tf_op jit(solution)/shard_map/dot_general | solution.py:156
  212.6 16.8 %reduce-scatter.2.cloned.1.call-done = bf16[512,2048]{1,0:T(8,128)(2,1)} async-done(((bf16[1024,2048]{1,0:T(8,128)(2,1)}), bf16[512,2048]{1,0:T(8,128)(2,1)}) %reduce-scatter.2.cloned.1.call-update) | async-done | bytes 2097168 | tf_op jit(solution)/shard_map/reduce_scatter | solution.py:160
  (172 shorter events, 100.9 us)
Async XLA Ops:
  6.5 187.3 %copy-start = (bf16[512,2048]{1,0:T(8,128)(2,1)S(1)}, bf16[512,2048]{1,0:T(8,128)(2,1)}, u32[]{:S(2)}) copy-start(bf16[512,2048]{1,0:T(8,128)(2,1)} %param.28) | copy-start | bytes 6291460
  6.5 20.4 %all-gather.2.cloned.1.call-start = ((), (), s32[]{:S(2)}) async-start(), calls=%async_computation.1 | async-start | bytes 6291456 | tf_op jit(solution)/shard_map/all_gather | solution.py:87
  6.5 2.4 %copy-start.3 = (bf16[512,2048]{1,0:T(8,128)(2,1)S(1)}, bf16[512,2048]{1,0:T(8,128)(2,1)}, u32[]{:S(2)}) copy-start(bf16[512,2048]{1,0:T(8,128)(2,1)} %param.17) | copy-start | bytes 6291460
  11.5 217.9 %reduce-scatter.2.cloned.1.call-start = ((), (), s32[]{:S(2)}) async-start(), calls=%async_computation.2 | async-start | bytes 6291456 | tf_op jit(solution)/shard_map/reduce_scatter | solution.py:160
  27.0 6.8 %copy-start.27 = (bf16[1024,2048]{1,0:T(8,128)(2,1)S(1)}, bf16[1024,2048]{1,0:T(8,128)(2,1)}, u32[]{:S(2)}) copy-start(bf16[1024,2048]{1,0:T(8,128)(2,1)} %all-gather.2.cloned.1.call-done) | copy-start | bytes 12582916
  27.0 6.8 %copy-start.28 = (bf16[2048,512]{1,0:T(8,128)(2,1)S(1)}, bf16[2048,512]{1,0:T(8,128)(2,1)}, u32[]{:S(2)}) copy-start(bf16[2048,512]{1,0:T(8,128)(2,1)} %param.21) | copy-start | bytes 6291460
  32.3 4.0 %copy-start.5 = (bf16[1024,512]{1,0:T(8,128)(2,1)}, bf16[1024,512]{1,0:T(8,128)(2,1)S(1)}, u32[]{:S(2)}) copy-start(bf16[1024,512]{1,0:T(8,128)(2,1)S(1)} %convolution_convert_fusion.4) | copy-start | bytes 3145732
  32.3 153.8 %collective-permute-start.1 = (bf16[16,512]{1,0:T(8,128)(2,1)S(1)}, bf16[16,512]{1,0:T(8,128)(2,1)S(1)}, u32[]{:S(2)}, u32[]{:S(2)}) collective-permute-start(bf16[16,512]{1,0:T(8,128)(2,1)S(1)} %slice.85), channel_id=1, source_target_pairs={{0,8},{8,16},{16,24},{1,9},{9,17},{17,25},{2,10},{10,18},{18,26},{... | collective-permute-start | bytes 49160 | tf_op jit(solution)/shard_map/ppermute | solution.py:17
  78.3 3.4 %copy-start.1 = (f32[1024,4,64]{2,0,1:T(8,128)S(1)}, f32[1024,4,64]{2,0,1:T(8,128)}, u32[]{:S(2)}) copy-start(f32[1024,4,64]{2,0,1:T(8,128)} %get-tuple-element.270) | copy-start | bytes 3145732
  78.3 3.4 %copy-start.2 = (f32[1024,4,64]{2,0,1:T(8,128)S(1)}, f32[1024,4,64]{2,0,1:T(8,128)}, u32[]{:S(2)}) copy-start(f32[1024,4,64]{2,0,1:T(8,128)} %get-tuple-element.271) | copy-start | bytes 3145732
  81.7 1.9 copy-start.4
  155.2 7.4 %collective-permute-start = (bf16[4,128,128]{2,1,0:T(8,128)(2,1)S(1)}, bf16[4,128,128]{2,1,0:T(8,128)(2,1)S(1)}, u32[]{:S(2)}, u32[]{:S(2)}) collective-permute-start(bf16[4,128,128]{2,1,0:T(8,128)(2,1)S(1)} %get-tuple-element.462), channel_id=1, source_target_pairs={{0,8},{8,16},{16,24},{1,9},{9,17},{17,25},{2,10},{10,18},{18,26},{... | collective-permute-start | bytes 393224 | tf_op jit(solution)/shard_map/while/body/eval_jaxpr/ppermute | solution.py:17
  163.3 5.7 %collective-permute-start = (bf16[4,128,128]{2,1,0:T(8,128)(2,1)S(1)}, bf16[4,128,128]{2,1,0:T(8,128)(2,1)S(1)}, u32[]{:S(2)}, u32[]{:S(2)}) collective-permute-start(bf16[4,128,128]{2,1,0:T(8,128)(2,1)S(1)} %get-tuple-element.462), channel_id=1, source_target_pairs={{0,8},{8,16},{16,24},{1,9},{9,17},{17,25},{2,10},{10,18},{18,26},{... | collective-permute-start | bytes 393224 | tf_op jit(solution)/shard_map/while/body/eval_jaxpr/ppermute | solution.py:17
  169.8 5.7 %collective-permute-start = (bf16[4,128,128]{2,1,0:T(8,128)(2,1)S(1)}, bf16[4,128,128]{2,1,0:T(8,128)(2,1)S(1)}, u32[]{:S(2)}, u32[]{:S(2)}) collective-permute-start(bf16[4,128,128]{2,1,0:T(8,128)(2,1)S(1)} %get-tuple-element.462), channel_id=1, source_target_pairs={{0,8},{8,16},{16,24},{1,9},{9,17},{17,25},{2,10},{10,18},{18,26},{... | collective-permute-start | bytes 393224 | tf_op jit(solution)/shard_map/while/body/eval_jaxpr/ppermute | solution.py:17
  183.0 3.2 %copy-start.6 = (bf16[1024,512]{1,0:T(8,128)(2,1)S(1)}, bf16[1024,512]{1,0:T(8,128)(2,1)}, u32[]{:S(2)}) copy-start(bf16[1024,512]{1,0:T(8,128)(2,1)} %copy-done.5) | copy-start | bytes 3145732
  186.0 0.7 copy-start.11
  186.0 0.7 copy-start.12
  186.0 0.7 copy-start.13
  186.0 0.7 copy-start.14
  186.0 0.7 copy-start.18
  186.8 6.2 %copy-start.7 = (bf16[2,256,256]{2,1,0:T(8,128)(2,1)S(1)}, bf16[2,256,256]{2,1,0:T(8,128)(2,1)}, u32[]{:S(2)}) copy-start(bf16[2,256,256]{2,1,0:T(8,128)(2,1)} %param.24) | copy-start | bytes 786436
  186.8 6.2 %copy-start.9 = (f32[2,256]{1,0:T(2,128)S(1)}, f32[2,256]{1,0:T(2,128)}, u32[]{:S(2)}) copy-start(f32[2,256]{1,0:T(2,128)} %param.25) | copy-start | bytes 6148
  192.9 0.7 copy-start.10
  193.8 5.7 %copy-start.29 = (f32[512]{0:T(512)S(1)}, f32[512]{0:T(512)}, u32[]{:S(2)}) copy-start(f32[512]{0:T(512)} %param.27) | copy-start | bytes 6148
  (12 other events, 8.0 us)
Sparse Core Ops, SparseCore 0:
  11.6 15.3 all-gather.1
  212.7 16.5 reduce-scatter.1
where the time goes:
time: 239 us; the launch traced here: 236 us
  matrix products  92.8 us (39%)
  local copies, waits for them, and re-layouts  49.6 us (21%)
  waiting for transfers between devices  38.5 us (16%)
  other arithmetic  35.6 us (15%)
  between operations  13.9 us (6%)
  starting transfers between devices  5.37 us (2%)
    dot_general x4, matrix products, per_device(): jnp.dot(piece, weight, preferred_element_type=jnp.float32)  19.6 us
    reduce_scatter x1, waiting for transfers between devices, per_device(): lax.psum_scatter(rounded.astype(jnp.float32).astype(jnp.bfloat16), 'tp',...  16.8 us
    dot_general x8, matrix products, advance(): jnp.einsum('hid,hde->hie', qb, state, precision=hp)  16.5 us
    ppermute x4, waiting for transfers between devices, shifted(): return lax.ppermute(array, axis, pairs)  14.8 us
    dynamic_slice x8, local copies, waits for them, and re-layouts, retain(): lax.scan(advance, start, (split(query), split(key), split(value)))  14.2 us
    dot_general x1, matrix products, per_device(): jnp.dot(ret_out, w_out_ret, preferred_element_type=jnp.float32)  13.1 us
    unnamed x64, local copies, waits for them, and re-layouts  12.2 us
    dot_general x8, matrix products, advance(): scores = jnp.einsum('hid,hjd->hij', qb, kb, precision=hp) * inner  11 us
  transfers between devices with their start and end apart: 6, of which 5 were waited for; matrix products, arithmetic and copies ran while one was open for 60% of the time, Pallas kernels for 0%

commit v1 on v0

v1 whole, which is shorter than its diff:
```python
import functools
import math

import jax
import jax.numpy as jnp
from jax import lax
from jax.experimental import pallas as pl
from jax.experimental.pallas import tpu as pltpu
from jax.sharding import PartitionSpec as P

GROUP_DIM = 256
HEAD_DIM = 128
CHUNK = 256
SUB = 128
RIM = 16
F32 = jnp.float32
BF16 = jnp.bfloat16


def dot(a, b):
    return jnp.dot(a, b, preferred_element_type=F32)


def layer_kernel(
    n_sp,
    n_tp,
    tokens,
    norm_gain,
    w_pool,
    w_query,
    w_key,
    w_value,
    w_gate,
    pool_mix,
    pool_bias,
    pool_gain,
    ret_gain,
    w_out_pool,
    w_out_ret,
    out,
    tok,
    wts,
    pr,
    wo,
    kr,
    qr,
    raw,
    cat,
    cosine,
    sine,
    decay,
    qdec,
    kdec,
    states,
    total,
    sin_buf,
    sout_buf,
    band,
    part_send,
    part_recv,
    out_buf,
    tok_sem,
    w_sem,
    wo_sem,
    tok_rs,
    st_send,
    st_recv,
    rim_rs,
    part_ss,
    part_rs,
    out_sem,
):
    tp = lax.axis_index("tp")
    sp = lax.axis_index("sp")
    rows = tokens.shape[0]
    length = rows * n_tp
    width = w_query.shape[1]
    wide = wo.shape[1]
    heads = width // HEAD_DIM
    groups = w_pool.shape[1] // GROUP_DIM
    chunks = length // CHUNK
    seq_len = length * n_sp
    own = pl.multiple_of(tp * rows, rows)
    other = pl.multiple_of((n_tp - 1 - tp) * rows, rows)
    peer = {"tp": n_tp - 1 - tp}

    tok_in = pltpu.make_async_copy(tokens, tok.at[pl.ds(own, rows)], tok_sem)
    tok_in.start()
    w_in = [
        pltpu.make_async_copy(w, wts.at[i], w_sem.at[i])
        for i, w in enumerate((w_key, w_value, w_pool, w_query, w_gate))
    ]
    for copy in w_in:
        copy.start()
    half = w_out_pool.shape[0]
    wo_in = [
        pltpu.make_async_copy(w_out_pool, wo.at[pl.ds(0, half)], wo_sem.at[0]),
        pltpu.make_async_copy(w_out_ret, wo.at[pl.ds(half, width)], wo_sem.at[1]),
    ]
    for copy in wo_in:
        copy.start()

    barrier = pltpu.get_barrier_semaphore()
    pl.semaphore_signal(barrier, inc=1, device_id=peer, device_id_type=pl.DeviceIdType.MESH)

    @pl.when(sp > 0)
    def _():
        pl.semaphore_signal(
            barrier, inc=1, device_id={"sp": sp - 1}, device_id_type=pl.DeviceIdType.MESH
        )

    @pl.when(sp < n_sp - 1)
    def _():
        pl.semaphore_signal(
            barrier, inc=1, device_id={"sp": sp + 1}, device_id_type=pl.DeviceIdType.MESH
        )

    neighbours = jnp.where(sp > 0, 1, 0) + jnp.where(sp < n_sp - 1, 1, 0)
    pl.semaphore_wait(barrier, 1 + neighbours)

    tok_out = pltpu.make_async_remote_copy(
        src_ref=tokens,
        dst_ref=tok.at[pl.ds(own, rows)],
        send_sem=tok_rs.at[0],
        recv_sem=tok_rs.at[1],
        device_id=peer,
        device_id_type=pl.DeviceIdType.MESH,
    )
    tok_out.start()

    def log_decay(h):
        total_heads = heads * n_tp
        value = jnp.float32(0.0)
        for t in range(n_tp):
            one = -(2.0**-5) * (seq_len / 16.0) ** (-2.0 * (t * heads + h) / (total_heads - 1))
            value = jnp.where(tp == t, jnp.float32(one), value)
        return value

    logs = [log_decay(h) for h in range(heads)]
    lane = lax.broadcasted_iota(jnp.int32, (SUB, HEAD_DIM), 1)
    row = lax.broadcasted_iota(jnp.int32, (SUB, HEAD_DIM), 0)
    hd = HEAD_DIM // 2
    low = lane < hd
    freq = jnp.exp(
        jnp.where(low, lane, lane - hd).astype(F32) * (-math.log(10000.0) / hd)
    )
    ang = row.astype(F32) * freq
    cos_r, sin_r = jnp.cos(ang), jnp.sin(ang)
    subs = length // SUB
    base_row = lax.broadcasted_iota(jnp.int32, (subs, HEAD_DIM), 0)
    base = (sp * length + base_row * SUB).astype(F32) * freq[:subs]
    cos_b, sin_b = jnp.cos(base), jnp.sin(base)
    for b in range(subs):
        cb, sb = cos_b[b : b + 1], sin_b[b : b + 1]
        cosine[b * SUB : (b + 1) * SUB] = cb * cos_r - sb * sin_r
        s = sb * cos_r + cb * sin_r
        sine[b * SUB : (b + 1) * SUB] = jnp.where(low, -s, s)

    step_i = lax.broadcasted_iota(jnp.int32, (CHUNK, HEAD_DIM), 0).astype(F32)
    di = lax.broadcasted_iota(jnp.int32, (CHUNK, CHUNK), 0) - lax.broadcasted_iota(
        jnp.int32, (CHUNK, CHUNK), 1
    )
    dpos = jnp.maximum(di, 0).astype(F32)
    for h in range(heads):
        decay[h] = jnp.where(di >= 0, jnp.exp(logs[h] * dpos), 0.0)
        qdec[h] = jnp.exp(logs[h] * (step_i + 1.0))
        kdec[h] = jnp.exp(logs[h] * (CHUNK - 1.0 - step_i))
    bi = lax.broadcasted_iota(jnp.int32, (SUB, SUB + RIM), 0)
    bj = lax.broadcasted_iota(jnp.int32, (SUB, SUB + RIM), 1)
    back = bi + RIM - bj
    windows = [jnp.left_shift(jnp.int32(2), tp * groups + g) for g in range(groups)]
    for g in range(groups):
        band[g] = jnp.where((back >= 0) & (back < windows[g]), 1.0, 0.0).astype(BF16)

    @pl.when(sp == 0)
    def _():
        pr[2, 0:RIM] = jnp.zeros((RIM, width), BF16)
        sin_buf[...] = jnp.zeros_like(sin_buf)

    def norm_rows(start):
        step = 16

        def body(i, carry):
            at = pl.ds(pl.multiple_of(start + i * step, step), step)
            x = tok[at, :].astype(F32)
            scale = lax.rsqrt(jnp.mean(x * x, axis=-1, keepdims=True) + 1e-06)
            tok[at, :] = (x * scale * norm_gain[...]).astype(BF16)
            return carry

        lax.fori_loop(0, rows // step, body, 0)

    def project(w, start):
        start = pl.multiple_of(start, CHUNK)
        res = dot(tok[pl.ds(start, CHUNK), :], wts[w])
        pr[w, pl.ds(pl.multiple_of(start + RIM, RIM), CHUNK)] = res.astype(BF16)

    per_half = rows // CHUNK

    def kv_half(start):
        def body(i, carry):
            project(i // per_half, start + (i % per_half) * CHUNK)
            return carry

        lax.fori_loop(0, 2 * per_half, body, 0)

    tok_in.wait()
    norm_rows(own)
    w_in[0].wait()
    w_in[1].wait()
    kv_half(own)
    tok_out.wait_recv()
    norm_rows(other)
    kv_half(other)

    def rotate(x, at):
        return x * cosine[at] + pltpu.roll(x, HEAD_DIM // 2, 1) * sine[at]

    for h in range(heads):
        total[h] = jnp.zeros((HEAD_DIM, HEAD_DIM), F32)
    block_decays = [jnp.exp(jnp.full((1, HEAD_DIM), logs[h] * CHUNK, F32)) for h in range(heads)]
    length_decays = [jnp.exp(jnp.full((1, HEAD_DIM), logs[h] * length, F32)) for h in range(heads)]

    def state_body(b, carry):
        at = pl.ds(pl.multiple_of(b * CHUNK, CHUNK), CHUNK)
        pat = pl.ds(pl.multiple_of(b * CHUNK + RIM, RIM), CHUNK)
        for h in range(heads):
            cols = slice(h * HEAD_DIM, (h + 1) * HEAD_DIM)
            k = rotate(pr[0, pat, cols].astype(F32), at) * HEAD_DIM**-0.5
            kr[at, cols] = k.astype(BF16)
            kd = (k * kdec[h]).astype(BF16)
            new = lax.dot_general(
                kd, pr[1, pat, cols], (((0,), (0,)), ((), ())), preferred_element_type=F32
            )
            states[b, h] = total[h]
            total[h] = total[h] * block_decays[h] + new
        return carry

    lax.fori_loop(0, chunks, state_body, 0)
    for copy in w_in[2:]:
        copy.wait()

    slots = 3 * chunks + chunks
    st_copies = [
        pltpu.make_async_remote_copy(
            src_ref=sout_buf.at[h],
            dst_ref=sin_buf.at[h],
            send_sem=st_send.at[h],
            recv_sem=st_recv.at[h],
            device_id={"sp": sp + 1},
            device_id_type=pl.DeviceIdType.MESH,
        )
        for h in range(heads)
    ]
    rim_copy = pltpu.make_async_remote_copy(
        src_ref=pr.at[2, pl.ds(length, RIM)],
        dst_ref=pr.at[2, pl.ds(0, RIM)],
        send_sem=rim_rs.at[0],
        recv_sem=rim_rs.at[1],
        device_id={"sp": sp + 1},
        device_id_type=pl.DeviceIdType.MESH,
    )

    def relay(c):
        for h in range(heads):

            @pl.when(jnp.minimum(3 * sp + h, slots - 1) == c)
            def _():
                @pl.when(sp > 0)
                def _():
                    st_copies[h].wait_recv()

                @pl.when(sp < n_sp - 1)
                def _():
                    sout_buf[h] = (
                        total[h] + length_decays[h] * sin_buf[h].astype(F32)
                    ).astype(BF16)
                    st_copies[h].start()

    def proj_body(c, carry):
        relay(c)

        @pl.when((c == chunks) & (sp < n_sp - 1))
        def _():
            rim_copy.start()

        project(2 + c // chunks, (c % chunks) * CHUNK)
        return carry

    lax.fori_loop(0, 3 * chunks, proj_body, 0)

    @pl.when(sp > 0)
    def _():
        rim_copy.wait_recv()

    def local_body(b, carry):
        relay(3 * chunks + b)
        at = pl.ds(pl.multiple_of(b * CHUNK, CHUNK), CHUNK)
        pat = pl.ds(pl.multiple_of(b * CHUNK + RIM, RIM), CHUNK)
        for h in range(heads):
            cols = slice(h * HEAD_DIM, (h + 1) * HEAD_DIM)
            q = rotate(pr[3, pat, cols].astype(F32), at).astype(BF16)
            qr[at, cols] = q
            scores = lax.dot_general(
                q, kr[at, cols], (((1,), (1,)), ((), ())), preferred_element_type=F32
            )
            scores = (scores * decay[h]).astype(BF16)
            raw[at, cols] = dot(scores, pr[1, pat, cols]) + qdec[h] * dot(
                q, states[b, h].astype(BF16)
            )
        for s in range(CHUNK // SUB):
            first = b * CHUNK + s * SUB
            here = sp * length + first + lax.broadcasted_iota(jnp.int32, (SUB, GROUP_DIM), 0)
            for g in range(groups):
                cols = slice(g * GROUP_DIM, (g + 1) * GROUP_DIM)
                span = pr[2, pl.ds(pl.multiple_of(first, SUB), SUB + RIM), cols]
                x = pr[2, pl.ds(pl.multiple_of(first + RIM, RIM), SUB), cols].astype(F32)
                count = jnp.minimum(here + 1, windows[g]).astype(F32)
                diff = (dot(band[g], span) / count - x).astype(BF16)
                mixed = dot(diff, pool_mix[g]) + pool_bias[g : g + 1]
                cat[pl.ds(pl.multiple_of(first, SUB), SUB), cols] = (
                    mixed * pool_gain[:, cols]
                ).astype(BF16)
        return carry

    lax.fori_loop(0, chunks, local_body, 0)
    for copy in wo_in:
        copy.wait()

    def finish(start):
        at = pl.ds(pl.multiple_of(start, CHUNK), CHUNK)
        pat = pl.ds(pl.multiple_of(start + RIM, RIM), CHUNK)
        for h in range(heads):
            cols = slice(h * HEAD_DIM, (h + 1) * HEAD_DIM)
            ahead = jnp.exp(jnp.full((1, HEAD_DIM), logs[h], F32) * start.astype(F32))
            state = (sin_buf[h].astype(F32) * ahead).astype(BF16)
            r = raw[at, cols] + qdec[h] * dot(qr[at, cols], state)
            r = r - jnp.mean(r, axis=-1, keepdims=True)
            var = jnp.mean(r * r, axis=-1, keepdims=True)
            gate = pr[4, pat, cols].astype(F32)
            gated = gate * (1.0 / (1.0 + jnp.exp(-gate))) * ret_gain[:, cols]
            cat[at, half + h * HEAD_DIM : half + (h + 1) * HEAD_DIM] = (
                gated * (r * lax.rsqrt(var + 1e-06))
            ).astype(BF16)
        return at

    def part_copy(j):
        at = pl.ds(pl.multiple_of(j * CHUNK, CHUNK), CHUNK)
        return pltpu.make_async_remote_copy(
            src_ref=part_send.at[at],
            dst_ref=part_recv.at[at],
            send_sem=part_ss.at[j],
            recv_sem=part_rs.at[j],
            device_id=peer,
            device_id_type=pl.DeviceIdType.MESH,
        )

    def out_copy(j):
        at = pl.ds(pl.multiple_of(j * CHUNK, CHUNK), CHUNK)
        return pltpu.make_async_copy(out_buf.at[at], out.at[at], out_sem.at[j])

    tile = 512

    def send_body(j, carry):
        at = finish(other + j * CHUNK)
        mine = pl.ds(pl.multiple_of(j * CHUNK, CHUNK), CHUNK)
        for n in range(wide // tile):
            cols = slice(n * tile, (n + 1) * tile)
            part_send[mine, cols] = dot(cat[at, :], wo[:, cols]).astype(BF16)
        part_copy(j).start()
        return carry

    lax.fori_loop(0, per_half, send_body, 0)

    def own_body(j, carry):
        at = finish(own + j * CHUNK)
        mine = pl.ds(pl.multiple_of(j * CHUNK, CHUNK), CHUNK)
        part_copy(j).wait_recv()
        for n in range(wide // tile):
            cols = slice(n * tile, (n + 1) * tile)
            part = dot(cat[at, :], wo[:, cols]).astype(BF16).astype(F32)
            out_buf[mine, cols] = (part + part_recv[mine, cols].astype(F32)).astype(BF16)
        out_copy(j).start()
        return carry

    lax.fori_loop(0, per_half, own_body, 0)

    tok_out.wait_send()
    for j in range(per_half):
        part_copy(j).wait_send()
        out_copy(j).wait()

    @pl.when(sp < n_sp - 1)
    def _():
        rim_copy.wait_send()
        for h in range(heads):
            st_copies[h].wait_send()


def per_device(
    tokens,
    norm_gain,
    w_pool,
    w_query,
    w_key,
    w_value,
    w_gate,
    pool_mix,
    pool_bias,
    pool_gain,
    ret_gain,
    w_out_pool,
    w_out_ret,
):
    n_sp, n_tp = lax.axis_size("sp"), lax.axis_size("tp")
    rows, model = tokens.shape
    length = rows * n_tp
    width = w_query.shape[1]
    heads = width // HEAD_DIM
    pool_width = w_pool.shape[1]
    groups = pool_width // GROUP_DIM
    chunks = length // CHUNK
    per_half = rows // CHUNK
    wide = w_out_pool.shape[1]
    hbm = pl.BlockSpec(memory_space=pl.ANY)
    vmem = pl.BlockSpec(memory_space=pltpu.VMEM)
    dma = pltpu.SemaphoreType.DMA
    flops = 2 * length * model * (pool_width + 4 * width) + 2 * length * (pool_width + width) * wide
    return pl.pallas_call(
        functools.partial(layer_kernel, n_sp, n_tp),
        out_shape=jax.ShapeDtypeStruct((rows, wide), BF16),
        in_specs=[hbm, vmem, hbm, hbm, hbm, hbm, hbm, vmem, vmem, vmem, vmem, hbm, hbm],
        out_specs=hbm,
        scratch_shapes=[
            pltpu.VMEM((length, model), BF16),
            pltpu.VMEM((5, model, width), BF16),
            pltpu.VMEM((5, length + RIM, width), BF16),
            pltpu.VMEM((pool_width + width, wide), BF16),
            pltpu.VMEM((length, width), BF16),
            pltpu.VMEM((length, width), BF16),
            pltpu.VMEM((length, width), F32),
            pltpu.VMEM((length, pool_width + width), BF16),
            pltpu.VMEM((length, HEAD_DIM), F32),
            pltpu.VMEM((length, HEAD_DIM), F32),
            pltpu.VMEM((heads, CHUNK, CHUNK), F32),
            pltpu.VMEM((heads, CHUNK, HEAD_DIM), F32),
            pltpu.VMEM((heads, CHUNK, HEAD_DIM), F32),
            pltpu.VMEM((chunks, heads, HEAD_DIM, HEAD_DIM), F32),
            pltpu.VMEM((heads, HEAD_DIM, HEAD_DIM), F32),
            pltpu.VMEM((heads, HEAD_DIM, HEAD_DIM), BF16),
            pltpu.VMEM((heads, HEAD_DIM, HEAD_DIM), BF16),
            pltpu.VMEM((groups, SUB, SUB + RIM), BF16),
            pltpu.VMEM((rows, wide), BF16),
            pltpu.VMEM((rows, wide), BF16),
            pltpu.VMEM((rows, wide), BF16),
            dma,
            dma((5,)),
            dma((2,)),
            dma((2,)),
            dma((heads,)),
            dma((heads,)),
            dma((2,)),
            dma((per_half,)),
            dma((per_half,)),
            dma((per_half,)),
        ],
        compiler_params=pltpu.CompilerParams(
            collective_id=0, has_side_effects=True, vmem_limit_bytes=62 * 1024 * 1024
        ),
        cost_estimate=pl.CostEstimate(
            flops=flops, bytes_accessed=20 * 1024 * 1024, transcendentals=0
        ),
    )(
        tokens,
        norm_gain.reshape(1, -1),
        w_pool,
        w_query,
        w_key,
        w_value,
        w_gate,
        pool_mix,
        pool_bias,
        pool_gain.reshape(1, -1),
        ret_gain.reshape(1, -1),
        w_out_pool,
        w_out_ret,
    )


def solution(mesh):
    return jax.shard_map(
        per_device,
        mesh=mesh,
        in_specs=(
            P(("fs", "sp", "tp"), None),
            P(),
            P(None, "tp"),
            P(None, "tp"),
            P(None, "tp"),
            P(None, "tp"),
            P(None, "tp"),
            P("tp", None, None),
            P("tp", None),
            P("tp"),
            P("tp"),
            P("tp", None),
            P("tp", None),
        ),
        out_specs=P(("fs", "sp", "tp"), None),
        check_vma=False,
    )
```

time: 239 us -> 47.5 us (0.20); the launches traced: 236 us -> 47.3 us
  matrix products: 92.8 us -> 0 us
  local copies, waits for them, and re-layouts: 49.6 us -> 3.16 us
  Pallas kernels: 0 us -> 44.2 us
  waiting for transfers between devices: 38.5 us -> 0 us
  other arithmetic: 35.6 us -> 0 us
  between operations: 13.9 us -> 0.01 us
  starting transfers between devices: 5.37 us -> 0 us
    dot_general x40 -> x0, matrix products: 92.8 us -> none  [the longest x4 19.6 us: per_device(): jnp.dot(piece, weight, preferred_element_type=jnp.float32)]
    pallas_call x0 -> x1, Pallas kernels: none -> 44.2 us  [per_device(): pl.pallas_call(functools.partial(layer_kernel, n_sp, n_tp), out_shape=jax...]
    reduce_scatter x1 -> x0, waiting for transfers between devices: 16.8 us -> none  [per_device(): lax.psum_scatter(rounded.astype(jnp.float32).astype(jnp.bfloat16), 'tp',...]
    ppermute x4 -> x0, waiting for transfers between devices: 14.8 us -> none  [shifted(): return lax.ppermute(array, axis, pairs)]
    dynamic_slice x8 -> x0, local copies, waits for them, and re-layouts: 14.2 us -> none  [retain(): lax.scan(advance, start, (split(query), split(key), split(value)))]
    convert_element_type x6 -> x0, other arithmetic: 9.72 us -> none  [the longest x1 6.13 us: per_device(): diff = (window_sum / count - padded[rim_len:]).astype(jnp.bfloat16).resha...]
    transpose x3 -> x0, local copies, waits for them, and re-layouts: 9.27 us -> none  [the longest x2 6.38 us: split(): values.reshape(blocks, BLOCK, heads_here, HEAD_DIM).transpose(0, 2, 1, 3)]
    unnamed x64 -> x1, local copies, waits for them, and re-layouts: 12.2 us -> 3.16 us
  transfers between devices with their start and end apart: 6 -> 0, of which waited for: 5 -> 0; matrix products, arithmetic and copies ran while one was open for 60% -> 0% of each run, Pallas kernels for 0% -> 0%
where the time goes in v1:
time: 47.5 us; the launch traced here: 47.3 us
  Pallas kernels  44.2 us (93%)
  local copies, waits for them, and re-layouts  3.16 us (7%)
    pallas_call x1, Pallas kernels, per_device(): pl.pallas_call(functools.partial(layer_kernel, n_sp, n_tp), out_shape=jax...  44.2 us
    unnamed x1, local copies, waits for them, and re-layouts  3.16 us

profile of v1, /device:TPU:29, one launch (start us, length us, event | category | flops | bytes accessed | tf_op | source)
XLA Modules:
  0.0 47.3 jit_solution(9799660698301054304)
XLA Ops:
  0.0 44.2 %shard_map.127 = bf16[512,2048]{1,0:T(8,128)(2,1)} custom-call(bf16[512,2048]{1,0:T(8,128)(2,1)} %tokens.1, f32[1,2048]{1,0:T(1,128)} %bitcast.3, bf16[2048,512]{1,0:T(8,128)(2,1)} %w_pool.1, bf16[2048,512]{1,0:T(8,128)(2,1)} %w_query.1, bf16[2048,512]{1,0:T(8,128)(2,1)} %w_key.1, bf16[2048,512]{1,0:T(8,128)(2,1)} %w_value.1, bf16[2048,512]{1,0:T(8,128)(2,1)} %w_gate.1, ...), custom_call_target="tpu_custom_call" | custom-call | flops 15032385536 | bytes 20971520 | tf_op jit(solution)/shard_map/pallas_call | solution.py:428
  44.2 3.2 %copy.15 = bf16[512,2048]{1,0:T(8,128)(2,1)} copy(bf16[512,2048]{1,0:T(8,128)(2,1)} %shard_map.127) | data formatting | bytes 4194304

commit v2 on v1

--- a/solution.py
+++ b/solution.py
@@ -13,6 +13,7 @@
 CHUNK = 256
 SUB = 128
 RIM = 16
+HOP = 4
 F32 = jnp.float32
 BF16 = jnp.bfloat16
 
@@ -37,15 +38,22 @@
     ret_gain,
     w_out_pool,
     w_out_ret,
-    out,
+    out_own,
+    part_recv,
     tok,
     wts,
-    pr,
+    pk,
+    pv,
+    pp,
+    pq,
+    pg,
     wo,
     kr,
     qr,
     raw,
-    cat,
+    pool_out,
+    ret_a,
+    ret_b,
     cosine,
     sine,
     decay,
@@ -56,9 +64,8 @@
     sin_buf,
     sout_buf,
     band,
+    ldec,
     part_send,
-    part_recv,
-    out_buf,
     tok_sem,
     w_sem,
     wo_sem,
@@ -68,7 +75,6 @@
     rim_rs,
     part_ss,
     part_rs,
-    out_sem,
 ):
     tp = lax.axis_index("tp")
     sp = lax.axis_index("sp")
@@ -90,15 +96,13 @@
         pltpu.make_async_copy(w, wts.at[i], w_sem.at[i])
         for i, w in enumerate((w_key, w_value, w_pool, w_query, w_gate))
     ]
-    for copy in w_in:
-        copy.start()
+    w_in[0].start()
+    w_in[1].start()
     half = w_out_pool.shape[0]
     wo_in = [
         pltpu.make_async_copy(w_out_pool, wo.at[pl.ds(0, half)], wo_sem.at[0]),
         pltpu.make_async_copy(w_out_ret, wo.at[pl.ds(half, width)], wo_sem.at[1]),
     ]
-    for copy in wo_in:
-        copy.start()
 
     barrier = pltpu.get_barrier_semaphore()
     pl.semaphore_signal(barrier, inc=1, device_id=peer, device_id_type=pl.DeviceIdType.MESH)
@@ -114,19 +118,6 @@
         pl.semaphore_signal(
             barrier, inc=1, device_id={"sp": sp + 1}, device_id_type=pl.DeviceIdType.MESH
         )
-
-    neighbours = jnp.where(sp > 0, 1, 0) + jnp.where(sp < n_sp - 1, 1, 0)
-    pl.semaphore_wait(barrier, 1 + neighbours)
-
-    tok_out = pltpu.make_async_remote_copy(
-        src_ref=tokens,
-        dst_ref=tok.at[pl.ds(own, rows)],
-        send_sem=tok_rs.at[0],
-        recv_sem=tok_rs.at[1],
-        device_id=peer,
-        device_id_type=pl.DeviceIdType.MESH,
-    )
-    tok_out.start()
 
     def log_decay(h):
         total_heads = heads * n_tp
@@ -174,8 +165,21 @@
 
     @pl.when(sp == 0)
     def _():
-        pr[2, 0:RIM] = jnp.zeros((RIM, width), BF16)
+        pp[0:RIM] = jnp.zeros((RIM, width), BF16)
         sin_buf[...] = jnp.zeros_like(sin_buf)
+
+    neighbours = jnp.where(sp > 0, 1, 0) + jnp.where(sp < n_sp - 1, 1, 0)
+    pl.semaphore_wait(barrier, 1 + neighbours)
+
+    tok_out = pltpu.make_async_remote_copy(
+        src_ref=tokens,
+        dst_ref=tok.at[pl.ds(own, rows)],
+        send_sem=tok_rs.at[0],
+        recv_sem=tok_rs.at[1],
+        device_id=peer,
+        device_id_type=pl.DeviceIdType.MESH,
+    )
+    tok_out.start()
 
     def norm_rows(start):
         step = 16
@@ -187,23 +191,26 @@
             tok[at, :] = (x * scale * norm_gain[...]).astype(BF16)
             return carry
 
-        lax.fori_loop(0, rows // step, body, 0)
-
-    def project(w, start):
+        lax.fori_loop(0, rows // step, body, 0, unroll=4)
+
+    def project(w, dst, start, pad=0):
         start = pl.multiple_of(start, CHUNK)
         res = dot(tok[pl.ds(start, CHUNK), :], wts[w])
-        pr[w, pl.ds(pl.multiple_of(start + RIM, RIM), CHUNK)] = res.astype(BF16)
+        dst[pl.ds(pl.multiple_of(start + pad, RIM), CHUNK)] = res.astype(BF16)
 
     per_half = rows // CHUNK
 
     def kv_half(start):
         def body(i, carry):
-            project(i // per_half, start + (i % per_half) * CHUNK)
+            project(0, pk, start + i * CHUNK)
+            project(1, pv, start + i * CHUNK)
             return carry
 
-        lax.fori_loop(0, 2 * per_half, body, 0)
+        lax.fori_loop(0, per_half, body, 0)
 
     tok_in.wait()
+    for copy in w_in[2:] + wo_in:
+        copy.start()
     norm_rows(own)
     w_in[0].wait()
     w_in[1].wait()
@@ -218,18 +225,18 @@
     for h in range(heads):
         total[h] = jnp.zeros((HEAD_DIM, HEAD_DIM), F32)
     block_decays = [jnp.exp(jnp.full((1, HEAD_DIM), logs[h] * CHUNK, F32)) for h in range(heads)]
-    length_decays = [jnp.exp(jnp.full((1, HEAD_DIM), logs[h] * length, F32)) for h in range(heads)]
+    for h in range(heads):
+        ldec[h] = jnp.exp(jnp.full((8, HEAD_DIM), logs[h] * length, F32))
 
     def state_body(b, carry):
         at = pl.ds(pl.multiple_of(b * CHUNK, CHUNK), CHUNK)
-        pat = pl.ds(pl.multiple_of(b * CHUNK + RIM, RIM), CHUNK)
         for h in range(heads):
             cols = slice(h * HEAD_DIM, (h + 1) * HEAD_DIM)
-            k = rotate(pr[0, pat, cols].astype(F32), at) * HEAD_DIM**-0.5
+            k = rotate(pk[at, cols].astype(F32), at) * HEAD_DIM**-0.5
             kr[at, cols] = k.astype(BF16)
             kd = (k * kdec[h]).astype(BF16)
             new = lax.dot_general(
-                kd, pr[1, pat, cols], (((0,), (0,)), ((), ())), preferred_element_type=F32
+                kd, pv[at, cols], (((0,), (0,)), ((), ())), preferred_element_type=F32
             )
             states[b, h] = total[h]
             total[h] = total[h] * block_decays[h] + new
@@ -239,9 +246,10 @@
     for copy in w_in[2:]:
         copy.wait()
 
-    slots = 3 * chunks + chunks
-    st_copies = [
-        pltpu.make_async_remote_copy(
+    slots = 3 * chunks
+
+    def st_copy(h):
+        return pltpu.make_async_remote_copy(
             src_ref=sout_buf.at[h],
             dst_ref=sin_buf.at[h],
             send_sem=st_send.at[h],
@@ -249,62 +257,74 @@
             device_id={"sp": sp + 1},
             device_id_type=pl.DeviceIdType.MESH,
         )
-        for h in range(heads)
-    ]
+
     rim_copy = pltpu.make_async_remote_copy(
-        src_ref=pr.at[2, pl.ds(length, RIM)],
-        dst_ref=pr.at[2, pl.ds(0, RIM)],
+        src_ref=pp.at[pl.ds(length, RIM)],
+        dst_ref=pp.at[pl.ds(0, RIM)],
         send_sem=rim_rs.at[0],
         recv_sem=rim_rs.at[1],
         device_id={"sp": sp + 1},
         device_id_type=pl.DeviceIdType.MESH,
     )
 
+    def relay_head(h):
+        @pl.when(sp > 0)
+        def _():
+            st_copy(h).wait_recv()
+
+        @pl.when(sp < n_sp - 1)
+        def _():
+            sout_buf[h] = (total[h] + ldec[h, 0:1] * sin_buf[h].astype(F32)).astype(BF16)
+            st_copy(h).start()
+
     def relay(c):
+        h = c - HOP * sp
+
+        @pl.when((h >= 0) & (h < heads) & (sp > 0))
+        def _():
+            relay_head(h)
+
+    @pl.when(sp == 0)
+    def _():
         for h in range(heads):
-
-            @pl.when(jnp.minimum(3 * sp + h, slots - 1) == c)
-            def _():
-                @pl.when(sp > 0)
-                def _():
-                    st_copies[h].wait_recv()
-
-                @pl.when(sp < n_sp - 1)
-                def _():
-                    sout_buf[h] = (
-                        total[h] + length_decays[h] * sin_buf[h].astype(F32)
-                    ).astype(BF16)
-                    st_copies[h].start()
-
-    def proj_body(c, carry):
+            relay_head(h)
+
+    def pool_body(c, carry):
         relay(c)
-
-        @pl.when((c == chunks) & (sp < n_sp - 1))
+        project(2, pp, c * CHUNK, RIM)
+        return carry
+
+    lax.fori_loop(0, chunks, pool_body, 0)
+
+    def query_body(c, carry):
+        relay(chunks + c)
+
+        @pl.when((c == 1) & (sp < n_sp - 1))
         def _():
             rim_copy.start()
 
-        project(2 + c // chunks, (c % chunks) * CHUNK)
+        project(3, pq, c * CHUNK)
         return carry
 
-    lax.fori_loop(0, 3 * chunks, proj_body, 0)
+    lax.fori_loop(0, chunks, query_body, 0)
 
     @pl.when(sp > 0)
     def _():
         rim_copy.wait_recv()
 
     def local_body(b, carry):
-        relay(3 * chunks + b)
+        relay(2 * chunks + b)
+        project(4, pg, b * CHUNK)
         at = pl.ds(pl.multiple_of(b * CHUNK, CHUNK), CHUNK)
-        pat = pl.ds(pl.multiple_of(b * CHUNK + RIM, RIM), CHUNK)
         for h in range(heads):
             cols = slice(h * HEAD_DIM, (h + 1) * HEAD_DIM)
-            q = rotate(pr[3, pat, cols].astype(F32), at).astype(BF16)
+            q = rotate(pq[at, cols].astype(F32), at).astype(BF16)
             qr[at, cols] = q
             scores = lax.dot_general(
                 q, kr[at, cols], (((1,), (1,)), ((), ())), preferred_element_type=F32
             )
             scores = (scores * decay[h]).astype(BF16)
-            raw[at, cols] = dot(scores, pr[1, pat, cols]) + qdec[h] * dot(
+            raw[at, cols] = dot(scores, pv[at, cols]) + qdec[h] * dot(
                 q, states[b, h].astype(BF16)
             )
         for s in range(CHUNK // SUB):
@@ -312,23 +332,31 @@
             here = sp * length + first + lax.broadcasted_iota(jnp.int32, (SUB, GROUP_DIM), 0)
             for g in range(groups):
                 cols = slice(g * GROUP_DIM, (g + 1) * GROUP_DIM)
-                span = pr[2, pl.ds(pl.multiple_of(first, SUB), SUB + RIM), cols]
-                x = pr[2, pl.ds(pl.multiple_of(first + RIM, RIM), SUB), cols].astype(F32)
+                span = pp[pl.ds(pl.multiple_of(first, SUB), SUB + RIM), cols]
+                x = pp[pl.ds(pl.multiple_of(first + RIM, RIM), SUB), cols].astype(F32)
                 count = jnp.minimum(here + 1, windows[g]).astype(F32)
                 diff = (dot(band[g], span) / count - x).astype(BF16)
                 mixed = dot(diff, pool_mix[g]) + pool_bias[g : g + 1]
-                cat[pl.ds(pl.multiple_of(first, SUB), SUB), cols] = (
+                pool_out[pl.ds(pl.multiple_of(first, SUB), SUB), cols] = (
                     mixed * pool_gain[:, cols]
                 ).astype(BF16)
         return carry
 
     lax.fori_loop(0, chunks, local_body, 0)
+
+    def rest(h, carry):
+        @pl.when((h + HOP * sp >= slots) & (sp > 0))
+        def _():
+            relay_head(h)
+
+        return carry
+
+    lax.fori_loop(0, heads, rest, 0)
     for copy in wo_in:
         copy.wait()
 
-    def finish(start):
+    def finish(start, ret):
         at = pl.ds(pl.multiple_of(start, CHUNK), CHUNK)
-        pat = pl.ds(pl.multiple_of(start + RIM, RIM), CHUNK)
         for h in range(heads):
             cols = slice(h * HEAD_DIM, (h + 1) * HEAD_DIM)
             ahead = jnp.exp(jnp.full((1, HEAD_DIM), logs[h], F32) * start.astype(F32))
@@ -336,12 +364,11 @@
             r = raw[at, cols] + qdec[h] * dot(qr[at, cols], state)
             r = r - jnp.mean(r, axis=-1, keepdims=True)
             var = jnp.mean(r * r, axis=-1, keepdims=True)
-            gate = pr[4, pat, cols].astype(F32)
+            gate = pg[at, cols].astype(F32)
             gated = gate * (1.0 / (1.0 + jnp.exp(-gate))) * ret_gain[:, cols]
-            cat[at, half + h * HEAD_DIM : half + (h + 1) * HEAD_DIM] = (
+            ret[:, cols] = (
                 gated * (r * lax.rsqrt(var + 1e-06))
             ).astype(BF16)
-        return at
 
     def part_copy(j):
         at = pl.ds(pl.multiple_of(j * CHUNK, CHUNK), CHUNK)
@@ -354,46 +381,41 @@
             device_id_type=pl.DeviceIdType.MESH,
         )
 
-    def out_copy(j):
-        at = pl.ds(pl.multiple_of(j * CHUNK, CHUNK), CHUNK)
-        return pltpu.make_async_copy(out_buf.at[at], out.at[at], out_sem.at[j])
-
     tile = 512
 
-    def send_body(j, carry):
-        at = finish(other + j * CHUNK)
-        mine = pl.ds(pl.multiple_of(j * CHUNK, CHUNK), CHUNK)
+    def multiply(start, ret, dst, j):
+        at = pl.ds(pl.multiple_of(start, CHUNK), CHUNK)
+        mine = slice(j * CHUNK, (j + 1) * CHUNK)
+        left = jnp.concatenate([pool_out[at, :], ret[...]], axis=1)
         for n in range(wide // tile):
             cols = slice(n * tile, (n + 1) * tile)
-            part_send[mine, cols] = dot(cat[at, :], wo[:, cols]).astype(BF16)
-        part_copy(j).start()
-        return carry
-
-    lax.fori_loop(0, per_half, send_body, 0)
-
-    def own_body(j, carry):
-        at = finish(own + j * CHUNK)
-        mine = pl.ds(pl.multiple_of(j * CHUNK, CHUNK), CHUNK)
+            dst[mine, cols] = dot(left, wo[:, cols]).astype(BF16)
+
+    starts = [other + j * CHUNK for j in range(per_half)] + [
+        own + j * CHUNK for j in range(per_half)
+    ]
+    rets = (ret_a, ret_b)
+    finish(starts[0], ret_a)
+    for i, start in enumerate(starts):
+        sending = i < per_half
+        multiply(start, rets[i % 2], part_send if sending else out_own, i % per_half)
+        if i + 1 < len(starts):
+            finish(starts[i + 1], rets[(i + 1) % 2])
+        if sending:
+            part_copy(i).start()
+
+    for j in range(per_half):
         part_copy(j).wait_recv()
-        for n in range(wide // tile):
-            cols = slice(n * tile, (n + 1) * tile)
-            part = dot(cat[at, :], wo[:, cols]).astype(BF16).astype(F32)
-            out_buf[mine, cols] = (part + part_recv[mine, cols].astype(F32)).astype(BF16)
-        out_copy(j).start()
-        return carry
-
-    lax.fori_loop(0, per_half, own_body, 0)
 
     tok_out.wait_send()
     for j in range(per_half):
         part_copy(j).wait_send()
-        out_copy(j).wait()
 
     @pl.when(sp < n_sp - 1)
     def _():
         rim_copy.wait_send()
         for h in range(heads):
-            st_copies[h].wait_send()
+            st_copy(h).wait_send()
 
 
 def per_device(
@@ -421,24 +443,30 @@
     chunks = length // CHUNK
     per_half = rows // CHUNK
     wide = w_out_pool.shape[1]
-    hbm = pl.BlockSpec(memory_space=pl.ANY)
+    hbm = pl.BlockSpec(memory_space=pltpu.HBM)
     vmem = pl.BlockSpec(memory_space=pltpu.VMEM)
     dma = pltpu.SemaphoreType.DMA
     flops = 2 * length * model * (pool_width + 4 * width) + 2 * length * (pool_width + width) * wide
-    return pl.pallas_call(
+    own, received = pl.pallas_call(
         functools.partial(layer_kernel, n_sp, n_tp),
-        out_shape=jax.ShapeDtypeStruct((rows, wide), BF16),
+        out_shape=[pltpu.VMEM((rows, wide), BF16)] * 2,
         in_specs=[hbm, vmem, hbm, hbm, hbm, hbm, hbm, vmem, vmem, vmem, vmem, hbm, hbm],
-        out_specs=hbm,
+        out_specs=[vmem, vmem],
         scratch_shapes=[
             pltpu.VMEM((length, model), BF16),
             pltpu.VMEM((5, model, width), BF16),
-            pltpu.VMEM((5, length + RIM, width), BF16),
+            pltpu.VMEM((length, width), BF16),
+            pltpu.VMEM((length, width), BF16),
+            pltpu.VMEM((length + RIM, pool_width), BF16),
+            pltpu.VMEM((length, width), BF16),
+            pltpu.VMEM((length, width), BF16),
             pltpu.VMEM((pool_width + width, wide), BF16),
             pltpu.VMEM((length, width), BF16),
             pltpu.VMEM((length, width), BF16),
             pltpu.VMEM((length, width), F32),
-            pltpu.VMEM((length, pool_width + width), BF16),
+            pltpu.VMEM((length, pool_width), BF16),
+            pltpu.VMEM((CHUNK, width), BF16),
+            pltpu.VMEM((CHUNK, width), BF16),
             pltpu.VMEM((length, HEAD_DIM), F32),
             pltpu.VMEM((length, HEAD_DIM), F32),
             pltpu.VMEM((heads, CHUNK, CHUNK), F32),
@@ -449,8 +477,7 @@
             pltpu.VMEM((heads, HEAD_DIM, HEAD_DIM), BF16),
             pltpu.VMEM((heads, HEAD_DIM, HEAD_DIM), BF16),
             pltpu.VMEM((groups, SUB, SUB + RIM), BF16),
-            pltpu.VMEM((rows, wide), BF16),
-            pltpu.VMEM((rows, wide), BF16),
+            pltpu.VMEM((heads, 8, HEAD_DIM), F32),
             pltpu.VMEM((rows, wide), BF16),
             dma,
             dma((5,)),
@@ -461,10 +488,9 @@
             dma((2,)),
             dma((per_half,)),
             dma((per_half,)),
-            dma((per_half,)),
         ],
         compiler_params=pltpu.CompilerParams(
-            collective_id=0, has_side_effects=True, vmem_limit_bytes=62 * 1024 * 1024
+            collective_id=0, has_side_effects=True, vmem_limit_bytes=50 * 1024 * 1024
         ),
         cost_estimate=pl.CostEstimate(
             flops=flops, bytes_accessed=20 * 1024 * 1024, transcendentals=0
@@ -484,6 +510,7 @@
         w_out_pool,
         w_out_ret,
     )
+    return (own.astype(F32) + received.astype(F32)).astype(BF16)
 
 
 def solution(mesh):

time: 47.5 us -> 40.3 us (0.85)
  Pallas kernels: 44.2 us -> 38 us
  local copies, waits for them, and re-layouts: 3.16 us -> 0 us
  other arithmetic: 0 us -> 2.24 us
    pallas_call x1, Pallas kernels: 44.2 us -> 38 us  [per_device(): pl.pallas_call(functools.partial(layer_kernel, n_sp, n_tp), out_shape=[pl...]
    unnamed x1 -> x0, local copies, waits for them, and re-layouts: 3.16 us -> none
    convert_element_type x0 -> x1, other arithmetic: none -> 2.24 us  [per_device(): return (own.astype(F32) + received.astype(F32)).astype(BF16)]
where the time goes in v2:
time: 40.3 us; the launch traced here: 40.2 us
  Pallas kernels  38 us (94%)
  other arithmetic  2.24 us (6%)
    pallas_call x1, Pallas kernels, per_device(): pl.pallas_call(functools.partial(layer_kernel, n_sp, n_tp), out_shape=[pl...  38 us
    convert_element_type x1, other arithmetic, per_device(): return (own.astype(F32) + received.astype(F32)).astype(BF16)  2.24 us

profile of v2, /device:TPU:29, one launch (start us, length us, event | category | flops | bytes accessed | tf_op | source)
XLA Modules:
  0.0 40.2 jit_solution(6372166304056341831)
XLA Ops:
  0.0 38.0 %shard_map.127 = (bf16[512,2048]{1,0:T(8,128)(2,1)S(1)}, bf16[512,2048]{1,0:T(8,128)(2,1)S(1)}) custom-call(bf16[512,2048]{1,0:T(8,128)(2,1)} %tokens.1, f32[1,2048]{1,0:T(1,128)} %bitcast.3, bf16[2048,512]{1,0:T(8,128)(2,1)} %w_pool.1, bf16[2048,512]{1,0:T(8,128)(2,1)} %w_query.1, bf16[2048,512]{1,0:T(8,128)(2,1)} %w_key.1, bf16[2048,512]{1,0:T(8,128)(2,1)} %w_value.1, ...), custom_call_target="tpu_custom_call" | custom-call | flops 15032385536 | bytes 20971520 | tf_op jit(solution)/shard_map/pallas_call | solution.py:450
  38.0 2.2 %add_convert_fusion = bf16[512,2048]{1,0:T(8,128)(2,1)} fusion(bf16[512,2048]{1,0:T(8,128)(2,1)S(1)} %get-tuple-element.8, bf16[512,2048]{1,0:T(8,128)(2,1)S(1)} %get-tuple-element.7), kind=kLoop, calls=%fused_computation | loop fusion | flops 4194304 | bytes 6291456 | tf_op jit(solution)/shard_map/convert_element_type | solution.py:513

commit v3 on v2

--- a/solution.py
+++ b/solution.py
@@ -13,7 +13,8 @@
 CHUNK = 256
 SUB = 128
 RIM = 16
-HOP = 4
+HOP = 2
+PARTS = 4
 F32 = jnp.float32
 BF16 = jnp.bfloat16
 
@@ -69,6 +70,7 @@
     tok_sem,
     w_sem,
     wo_sem,
+    tok_ss,
     tok_rs,
     st_send,
     st_recv,
@@ -171,15 +173,18 @@
     neighbours = jnp.where(sp > 0, 1, 0) + jnp.where(sp < n_sp - 1, 1, 0)
     pl.semaphore_wait(barrier, 1 + neighbours)
 
-    tok_out = pltpu.make_async_remote_copy(
-        src_ref=tokens,
-        dst_ref=tok.at[pl.ds(own, rows)],
-        send_sem=tok_rs.at[0],
-        recv_sem=tok_rs.at[1],
-        device_id=peer,
-        device_id_type=pl.DeviceIdType.MESH,
-    )
-    tok_out.start()
+    part = rows // PARTS
+
+    def tok_copy(i):
+        at = pl.ds(pl.multiple_of(own + i * part, part), part)
+        return pltpu.make_async_remote_copy(
+            src_ref=tok.at[at],
+            dst_ref=tok.at[at],
+            send_sem=tok_ss.at[i],
+            recv_sem=tok_rs.at[i],
+            device_id=peer,
+            device_id_type=pl.DeviceIdType.MESH,
+        )
 
     def norm_rows(start):
         step = 16
@@ -191,7 +196,7 @@
             tok[at, :] = (x * scale * norm_gain[...]).astype(BF16)
             return carry
 
-        lax.fori_loop(0, rows // step, body, 0, unroll=4)
+        lax.fori_loop(0, part // step, body, 0, unroll=4)
 
     def project(w, dst, start, pad=0):
         start = pl.multiple_of(start, CHUNK)
@@ -211,12 +216,16 @@
     tok_in.wait()
     for copy in w_in[2:] + wo_in:
         copy.start()
-    norm_rows(own)
+    for i in range(PARTS):
+        norm_rows(own + i * part)
+        if i > 0:
+            tok_copy(i - 1).start()
     w_in[0].wait()
     w_in[1].wait()
+    tok_copy(PARTS - 1).start()
     kv_half(own)
-    tok_out.wait_recv()
-    norm_rows(other)
+    for i in range(PARTS):
+        tok_copy(i).wait_recv()
     kv_half(other)
 
     def rotate(x, at):
@@ -280,7 +289,7 @@
     def relay(c):
         h = c - HOP * sp
 
-        @pl.when((h >= 0) & (h < heads) & (sp > 0))
+        @pl.when((h >= 0) & (h < heads) & (sp > 0) & (sp < n_sp - 1))
         def _():
             relay_head(h)
 
@@ -345,7 +354,9 @@
     lax.fori_loop(0, chunks, local_body, 0)
 
     def rest(h, carry):
-        @pl.when((h + HOP * sp >= slots) & (sp > 0))
+        late = (h + HOP * sp >= slots) | (sp == n_sp - 1)
+
+        @pl.when(late & (sp > 0))
         def _():
             relay_head(h)
 
@@ -407,7 +418,8 @@
     for j in range(per_half):
         part_copy(j).wait_recv()
 
-    tok_out.wait_send()
+    for i in range(PARTS):
+        tok_copy(i).wait_send()
     for j in range(per_half):
         part_copy(j).wait_send()
 
@@ -482,7 +494,8 @@
             dma,
             dma((5,)),
             dma((2,)),
-            dma((2,)),
+            dma((PARTS,)),
+            dma((PARTS,)),
             dma((heads,)),
             dma((heads,)),
             dma((2,)),

time: 40.3 us -> 37.8 us (0.938)
  Pallas kernels: 38 us -> 35.4 us
    pallas_call x1, Pallas kernels: 38 us -> 35.4 us  [per_device(): pl.pallas_call(functools.partial(layer_kernel, n_sp, n_tp), out_shape=[pl...]
where the time goes in v3:
time: 37.8 us; the launch traced here: 37.7 us
  Pallas kernels  35.4 us (94%)
  other arithmetic  2.24 us (6%)
    pallas_call x1, Pallas kernels, per_device(): pl.pallas_call(functools.partial(layer_kernel, n_sp, n_tp), out_shape=[pl...  35.4 us
    convert_element_type x1, other arithmetic, per_device(): return (own.astype(F32) + received.astype(F32)).astype(BF16)  2.24 us

profile of v3, /device:TPU:29, one launch (start us, length us, event | category | flops | bytes accessed | tf_op | source)
XLA Modules:
  0.0 37.7 jit_solution(17421623466776403573)
XLA Ops:
  0.0 35.4 %shard_map.127 = (bf16[512,2048]{1,0:T(8,128)(2,1)S(1)}, bf16[512,2048]{1,0:T(8,128)(2,1)S(1)}) custom-call(bf16[512,2048]{1,0:T(8,128)(2,1)} %tokens.1, f32[1,2048]{1,0:T(1,128)} %bitcast.3, bf16[2048,512]{1,0:T(8,128)(2,1)} %w_pool.1, bf16[2048,512]{1,0:T(8,128)(2,1)} %w_query.1, bf16[2048,512]{1,0:T(8,128)(2,1)} %w_key.1, bf16[2048,512]{1,0:T(8,128)(2,1)} %w_value.1, ...), custom_call_target="tpu_custom_call" | custom-call | flops 15032385536 | bytes 20971520 | tf_op jit(solution)/shard_map/pallas_call | solution.py:462
  35.4 2.2 %add_convert_fusion = bf16[512,2048]{1,0:T(8,128)(2,1)} fusion(bf16[512,2048]{1,0:T(8,128)(2,1)S(1)} %get-tuple-element.8, bf16[512,2048]{1,0:T(8,128)(2,1)S(1)} %get-tuple-element.7), kind=kLoop, calls=%fused_computation | loop fusion | flops 4194304 | bytes 6291456 | tf_op jit(solution)/shard_map/convert_element_type | solution.py:526
